TPU v7x, 32 devices: a whole 2x2x4 slice. The times are simulated.
32 devices in a mesh: sp: 8 (over z, x), tp: 4 (over y, core).
Axes of the slice: x: 2, y: 2, z: 4, core: 2. Of those that a mesh axis runs over, the one named last changes fastest.
Arguments:
- prompt_tokens: bfloat16 [8192, 2048], P(('sp', 'tp')), may hold values from -8 to 8
- key_weight: bfloat16 [2048, 2048], P(None, 'tp'), may hold values from -0.125 to 0.125
- value_weight: bfloat16 [2048, 4096], P(None, 'tp'), may hold values from -0.125 to 0.125
- input_weight: bfloat16 [2048, 32], replicated, may hold values from -4 to 4
- forget_weight: bfloat16 [2048, 32], replicated, may hold values from -0.125 to 0.125
- forget_bias: float32 [32], replicated, as said below
- new_token: bfloat16 [2048], replicated, may hold values from -8 to 8
- new_query: bfloat16 [2048], P('tp'), may hold values from -6 to 6
Outputs:
- key_cache: bfloat16 [8192, 2048], P('sp', 'tp')
- value_cache: bfloat16 [8192, 4096], P('sp', 'tp')
- cache_weight: float32 [32, 8192], P('tp', 'sp')
- reading: float32 [4096], P('tp')
Inputs may be any that keep to these rules, and one draw needn't show every extreme that they name: `forget_bias`: every head's forget gate offset is 2 or more.
All inputs are finite; a program needn't handle non-finite values.
Results may differ from a plain program's by a relative error of at most 0.0058.
Values may be sent and summed in bfloat16 or wider, within the bound.
A program may use at most 64 MiB of HBM per device.

v0:
```python
import math

import jax
import jax.numpy as jnp
from jax import lax
from jax.sharding import PartitionSpec as P

DQK = 64
DV = 128


def prefix(array, axis, combine, identity):
    peers, here = (lax.axis_size(axis), lax.axis_index(axis))
    everything = lax.all_gather(array, axis)
    start = jnp.broadcast_to(jnp.asarray(identity, array.dtype), array.shape)

    def step(k, before):
        at = peers - 1 - k
        reached = at > here
        new = combine(before, everything[at])
        return jnp.where(reached, new, before)

    return lax.fori_loop(0, peers, step, start)


def add_pairs(earlier, later_part):
    return earlier + later_part


def body(
    prompt_tokens,
    key_weight,
    value_weight,
    input_weight,
    forget_weight,
    forget_bias,
    new_token,
    new_query,
):
    heads_dev = key_weight.shape[1] // DQK
    head_start = lax.axis_index("tp") * heads_dev
    gate_input = lax.dynamic_slice_in_dim(input_weight, head_start, heads_dev, 1)
    gate_forget = lax.dynamic_slice_in_dim(forget_weight, head_start, heads_dev, 1)
    forget_shift = lax.dynamic_slice_in_dim(forget_bias, head_start, heads_dev, 0)
    packed = jnp.concatenate([key_weight, value_weight, gate_input, gate_forget], axis=1)
    key_end = heads_dev * DQK
    value_end = heads_dev * (DQK + DV)
    projected = jnp.dot(
        lax.all_gather(prompt_tokens, "tp", axis=0, tiled=True),
        packed,
        preferred_element_type=jnp.float32,
    )
    key_cache = projected[:, :key_end].astype(jnp.bfloat16)
    value_cache = projected[:, key_end:value_end].astype(jnp.bfloat16)
    input_gate = projected[:, value_end : value_end + heads_dev]
    forget_pre = projected[:, value_end + heads_dev :]
    log_forget = jax.nn.log_sigmoid(forget_pre + forget_shift)
    block_total = jnp.sum(log_forget, axis=0)
    carried = prefix(block_total, "sp", add_pairs, jnp.zeros_like(block_total))
    log_weight = (
        input_gate + (block_total[None, :] - jnp.cumsum(log_forget, axis=0)) + carried[None, :]
    )
    peak_log = lax.pmax(jnp.max(log_weight, axis=0), "sp")
    cache_weight = jnp.transpose(jnp.exp(log_weight - peak_log[None, :]), (1, 0))
    new_key = jnp.dot(new_token, key_weight, preferred_element_type=jnp.float32).astype(
        jnp.bfloat16
    )
    new_value = jnp.dot(new_token, value_weight, preferred_element_type=jnp.float32).astype(
        jnp.bfloat16
    )
    new_gate = jnp.dot(new_token, gate_input, preferred_element_type=jnp.float32)
    new_forget = jax.nn.log_sigmoid(
        jnp.dot(new_token, gate_forget, preferred_element_type=jnp.float32) + forget_shift
    )
    stable_level = jnp.maximum(new_forget + peak_log, new_gate)
    rows = log_weight.shape[0]
    query_heads = new_query.reshape(heads_dev, DQK)
    key_heads = key_cache.reshape(rows, heads_dev, DQK)
    key_score = jnp.einsum(
        "shd,hd->sh", key_heads, query_heads, preferred_element_type=jnp.float32
    ) / math.sqrt(DQK)
    new_score = jnp.einsum(
        "hd,hd->h", new_key.reshape(heads_dev, DQK), query_heads, preferred_element_type=jnp.float32
    ) / math.sqrt(DQK)
    weighted = jnp.exp(new_forget[None, :] + log_weight - stable_level[None, :]) * key_score
    value_heads = value_cache.reshape(rows, heads_dev, DV)
    numer_part = jnp.einsum(
        "sh,she->he", weighted.astype(jnp.bfloat16), value_heads, preferred_element_type=jnp.float32
    )
    denom_part = jnp.sum(weighted, axis=0)
    numerator, denominator = lax.psum((numer_part, denom_part), "sp")
    own_term = jnp.exp(new_gate - stable_level) * new_score
    numerator = numerator + own_term[:, None] * new_value.reshape(heads_dev, DV).astype(jnp.float32)
    denominator = denominator + own_term
    reading = numerator / jnp.maximum(jnp.abs(denominator), 1.0)[:, None]
    return (key_cache, value_cache, cache_weight, reading.reshape(-1))


def solution(mesh):
    placed = (P(("sp", "tp"), None), P(None, "tp"), P(None, "tp"), P(), P(), P(), P(), P("tp"))
    return jax.shard_map(
        body,
        mesh=mesh,
        in_specs=placed,
        out_specs=(P("sp", "tp"), P("sp", "tp"), P("tp", "sp"), P("tp")),
        check_vma=False,
    )
```

profile of v0, /device:TPU:0, one launch (start us, length us, event | category | flops | bytes accessed | tf_op | source)
XLA Modules:
  0.0 138.1 jit_solution(2018318325805021415)
XLA Ops:
  7.2 0.7 all-gather.3.cloned.1.call-update
  7.9 0.8 reshape.54
  8.7 0.8 reshape.80
  9.5 0.7 reshape.65
  10.2 2.0 %fusion.20 = f32[1,512]{1,0:T(1,128)S(1)} fusion(bf16[2048,1]{0,1:T(2,128)(2,1)S(1)} %reshape.65, bf16[2048,512]{1,0:T(8,128)(2,1)} %param.11), kind=kOutput, calls=%fused_computation.43 | convolution fusion | flops 2097152 | bytes 2103296 | tf_op jit(solution)/shard_map/dot_general | solution.py:65
  12.2 0.7 dynamic_slice.21
  13.0 0.8 constant_dynamic-slice_fusion
  13.7 0.3 copy.18
  14.0 0.3 copy.17
  14.3 0.6 dynamic-slice
  15.5 10.7 %concatenate.3 = bf16[2048,1552]{1,0:T(8,128)(2,1)} concatenate(bf16[2048,512]{1,0:T(8,128)(2,1)S(1)} %copy-done, bf16[2048,1024]{1,0:T(8,128)(2,1)} %param.12, bf16[2048,8]{1,0:T(8,128)(2,1)S(1)} %copy.17, bf16[2048,8]{1,0:T(8,128)(2,1)S(1)} %copy.18), dimensions={1} | concatenate | bytes 12713984 | tf_op jit(solution)/shard_map/concatenate | solution.py:45
  26.3 0.1 fusion.13
  26.5 2.8 %fusion.21 = f32[1,1024]{1,0:T(1,128)S(1)} fusion(bf16[2048,1]{0,1:T(2,128)(2,1)S(1)} %reshape.65, bf16[2048,1024]{1,0:T(8,128)(2,1)} %param.12), kind=kOutput, calls=%fused_computation.44 | convolution fusion | flops 4194304 | bytes 4202496 | tf_op jit(solution)/shard_map/dot_general | solution.py:68
  29.3 17.5 %all-gather.3.cloned.1.call-done = bf16[1024,2048]{1,0:T(8,128)(2,1)} async-done(((bf16[256,2048]{1,0:T(8,128)(2,1)}), bf16[1024,2048]{1,0:T(8,128)(2,1)}) %all-gather.3.cloned.1.call-update) | async-done | bytes 4194320 | tf_op jit(solution)/shard_map/all_gather | solution.py:49
  46.8 13.5 %fusion.18 = (bf16[1024,1552]{0,1:T(8,128)(2,1)S(1)}, f32[1024,1552]{0,1:T(8,128)S(1)}) fusion(bf16[2048,1552]{1,0:T(8,128)(2,1)} %concatenate.3, bf16[1024,2048]{1,0:T(8,128)(2,1)} %all-gather.3.cloned.1.call-done), kind=kOutput, calls=%fused_computation.41 | convolution fusion | flops 6511149056 | bytes 20086784 | tf_op jit(solution)/shard_map/dot_general | solution.py:48
  60.4 0.2 slice.27
  60.5 0.2 negate_bitcast_fusion
  60.7 2.2 %copy-done.1 = f32[1024,1552]{0,1:T(8,128)} copy-done((f32[1024,1552]{0,1:T(8,128)}, f32[1024,1552]{0,1:T(8,128)S(1)}, u32[]{:S(2)}) %copy-start.1) | copy-done | bytes 6357016
  62.9 2.3 %reduce-window.6 = f32[8,8,128]{2,1,0:T(8,128)S(1)} reduce-window(f32[8,8,128]{2,1,0:T(8,128)S(1)} %copy.19, f32[]{:T(128)} %constant.72.clone.1), window={size=1x1x128 pad=0_0x0_0x127_0}, to_apply=%region_1.2 | reduce-window | flops 1040384 | bytes 65540 | tf_op jit(solution)/shard_map/reduce-window
  65.3 21.3 %all-reduce = f32[64]{0:T(128)S(1)} all-reduce(f32[64]{0:T(128)S(1)} %get-tuple-element.158), channel_id=2, replica_groups=mesh['sp'=8,'tp'=4] {'sp'}, use_global_device_ids=true, to_apply=%add | all-reduce | flops 64 | bytes 512
  86.7 0.3 while.16
  87.1 0.2 slice_reduce_fusion
  87.2 0.2 reduce-window.9
  87.4 1.0 fusion.15
  88.4 17.1 %pmax.7 = f32[8]{0:T(128)S(1)} all-reduce(f32[8]{0:T(128)S(1)} %get-tuple-element.150), channel_id=1, replica_groups=mesh['sp'=8,'tp'=4] {'sp'}, use_global_device_ids=true, to_apply=%region_6.7 | all-reduce | flops 8 | bytes 64 | tf_op jit(solution)/shard_map/pmax | solution.py:63
  105.5 1.3 copy.20
  106.8 2.5 %copy.21 = bf16[1024,1024]{1,0:T(8,128)(2,1)} copy(bf16[1024,1024]{0,1:T(8,128)(2,1)S(1)} %slice.27) | data formatting | bytes 4194304
  109.5 0.3 fusion.19
  109.8 0.8 fusion.14
  110.6 0.6 fusion.6
  111.2 19.4 %all-reduce.1 = (f32[8,128]{1,0:T(8,128)S(1)}, f32[8]{0:T(128)S(1)}) all-reduce(f32[8,128]{1,0:T(8,128)S(1)} %bitcast.85, f32[8]{0:T(128)S(1)} %get-tuple-element.154), channel_id=1, replica_groups=mesh['sp'=8,'tp'=4] {'sp'}, use_global_device_ids=true, to_apply=%region_7.8 | all-reduce | flops 1032 | bytes 8256 | tf_op jit(solution)/shard_map/psum | solution.py:91
  130.6 0.7 fusion.10
  (26 shorter events, 0.9 us)
Async XLA Ops:
  7.2 7.1 %copy-start.2 = (u32[32]{0:T(128)S(1)}, u32[32]{0:T(128)}, u32[]{:S(2)}) copy-start(u32[32]{0:T(128)} %constant.80) | copy-start | bytes 388
  7.2 8.4 %copy-start = (bf16[2048,512]{1,0:T(8,128)(2,1)S(1)}, bf16[2048,512]{1,0:T(8,128)(2,1)}, u32[]{:S(2)}) copy-start(bf16[2048,512]{1,0:T(8,128)(2,1)} %param.11) | copy-start | bytes 6291460
  7.2 39.6 %all-gather.3.cloned.1.call-start = ((), (), s32[]{:S(2)}) async-start(), calls=%async_computation | async-start | bytes 5242880 | tf_op jit(solution)/shard_map/all_gather | solution.py:49
  60.3 2.7 %copy-start.1 = (f32[1024,1552]{0,1:T(8,128)}, f32[1024,1552]{0,1:T(8,128)S(1)}, u32[]{:S(2)}) copy-start(f32[1024,1552]{0,1:T(8,128)S(1)} %get-tuple-element.160) | copy-start | bytes 19070980
Sparse Core Ops, SparseCore 0:
  9.6 37.1 all-gather.2
where the time goes:
time: 139 us; the launch traced here: 138 us
  blocking collectives  57.8 us (42%)
  local copies, waits for them, and re-layouts  22.2 us (16%)
  matrix products  19.5 us (14%)
  waiting for transfers between devices  18.1 us (13%)
  between operations  14.8 us (11%)
  other arithmetic  5.51 us (4%)
    unnamed x1, blocking collectives  21.3 us
    psum x1, blocking collectives, body(): numerator, denominator = lax.psum((numer_part, denom_part), 'sp')  19.4 us
    all_gather x1, waiting for transfers between devices, body(): lax.all_gather(prompt_tokens, 'tp', axis=0, tiled=True)  17.5 us
    pmax x1, blocking collectives, body(): peak_log = lax.pmax(jnp.max(log_weight, axis=0), 'sp')  17.1 us
    dot_general x1, matrix products, body(): jnp.dot(lax.all_gather(prompt_tokens, 'tp', axis=0, tiled=True), packed,...  13.5 us
    concatenate x1, local copies, waits for them, and re-layouts, body(): jnp.concatenate([key_weight, value_weight, gate_input, gate_forget], axis=1)  10.7 us
    unnamed x11, local copies, waits for them, and re-layouts  7.33 us
    dot_general x1, matrix products, body(): jnp.dot(new_token, value_weight, preferred_element_type=jnp.float32)  2.85 us
  transfers between devices with their start and end apart: 1, of which 1 were waited for; matrix products, arithmetic and copies ran while one was open for 15% of the time, Pallas kernels for 0%

commit v1 on v0

v1 whole, which is shorter than its diff:
```python
import functools
import math

import jax
import jax.numpy as jnp
from jax import lax
from jax.experimental import pallas as pl
from jax.experimental.pallas import tpu as pltpu
from jax.sharding import PartitionSpec as P

DQK = 64
DV = 128
PAD = 16
MESH = pl.DeviceIdType.MESH
NT = (((1,), (1,)), ((), ()))


def dot(a, b):
    return jnp.dot(a, b, preferred_element_type=jnp.float32)


def dot_nt(a, b):
    return lax.dot_general(a, b, NT, preferred_element_type=jnp.float32)


def log_sigmoid(x):
    return jnp.minimum(x, 0.0) - jnp.log1p(jnp.exp(-jnp.abs(x)))


def pieces_of(rows):
    return [(0, rows // 2), (rows // 2, rows // 4), (rows // 2 + rows // 4, rows // 4)]


def kernel(
    n_sp,
    n_tp,
    tok_hbm,
    kw_hbm,
    vw_hbm,
    wi_ref,
    wf_ref,
    fb_ref,
    nt_ref,
    nq_ref,
    k_out,
    v_out,
    cw_out,
    rd_out,
    tok,
    kw,
    vw,
    gnew,
    s1_src,
    s1,
    s2_src,
    s2,
    s3_src,
    s3,
    lwb,
    wexp,
    local_sem,
    near_sem,
    far_send,
    far_recv,
    fwd_send,
    fwd_recv,
    s1_send,
    s1_recv,
    s2_send,
    s2_recv,
    s3_send,
    s3_recv,
):
    sp, tp = lax.axis_index("sp"), lax.axis_index("tp")
    chips = n_tp // 2
    chip, core = tp // 2, tp % 2
    mate = chip * 2 + (1 - core)
    rows = tok.shape[1]
    heads = s2_src.shape[0]
    all_heads = wi_ref.shape[0]
    pieces = pieces_of(rows)

    load_tok = pltpu.make_async_copy(tok_hbm, tok.at[tp], local_sem.at[0])
    load_kw = pltpu.make_async_copy(kw_hbm, kw, local_sem.at[1])
    load_vw = pltpu.make_async_copy(vw_hbm, vw, local_sem.at[2])
    load_tok.start()
    load_kw.start()
    load_vw.start()

    barrier = pltpu.get_barrier_semaphore()
    for k in range(1, n_tp):
        pl.semaphore_signal(
            barrier, inc=1, device_id=(sp, (tp + k) % n_tp), device_id_type=MESH
        )
    for k in range(1, n_sp):
        pl.semaphore_signal(
            barrier, inc=1, device_id=((sp + k) % n_sp, tp), device_id_type=MESH
        )
    pl.semaphore_wait(barrier, n_tp - 1 + n_sp - 1)

    def remote(src, dst, send, recv, device):
        return pltpu.make_async_remote_copy(
            src_ref=src,
            dst_ref=dst,
            send_sem=send,
            recv_sem=recv,
            device_id=device,
            device_id_type=MESH,
        )

    def far_copy(k, j):
        at, size = pieces[j]
        there = ((chip + k) % chips) * 2 + core
        return remote(
            tok_hbm.at[pl.ds(at, size)],
            tok.at[tp, pl.ds(at, size)],
            far_send.at[k - 1, j],
            far_recv.at[k - 1, j],
            (sp, there),
        )

    def came_from(k):
        return (chip - k + chips) % chips

    def forward_copy(k, j):
        at, size = pieces[j]
        slot = came_from(k) * 2 + core
        return remote(
            tok.at[slot, pl.ds(at, size)],
            tok.at[slot, pl.ds(at, size)],
            fwd_send.at[k - 1, j],
            fwd_recv.at[k - 1, j],
            (sp, mate),
        )

    near = remote(tok_hbm, tok.at[tp], near_sem.at[0], near_sem.at[1], (sp, mate))
    for k in range(1, chips):
        far_copy(k, 0).start()
    near.start()

    row_iota = lax.broadcasted_iota(jnp.int32, (all_heads, all_heads), 0)
    col_iota = lax.broadcasted_iota(jnp.int32, (all_heads, all_heads), 1)
    shift = jnp.sum(jnp.where(row_iota == col_iota, fb_ref[...], 0.0), axis=1, keepdims=True)
    load_tok.wait()
    own = tok[tp]
    gate = dot_nt(wi_ref[...], own)
    log_forget = log_sigmoid(dot_nt(wf_ref[...], own) + shift)
    later = lax.broadcasted_iota(jnp.int32, (rows, rows), 0) > lax.broadcasted_iota(
        jnp.int32, (rows, rows), 1
    )
    decay = jnp.dot(
        log_forget,
        later.astype(jnp.float32),
        precision=lax.Precision.HIGHEST,
        preferred_element_type=jnp.float32,
    )
    relative = gate + decay
    total = jnp.broadcast_to(jnp.sum(log_forget, axis=1, keepdims=True), (all_heads, 128))
    for t in range(n_tp):
        part = slice(t * heads, (t + 1) * heads)
        s1_src[t, :, :rows] = relative[part]
        s1_src[t, :, rows:] = total[part]

    def s1_copy(k):
        there = (tp + k) % n_tp
        return remote(
            s1_src.at[there], s1.at[tp], s1_send.at[k - 1], s1_recv.at[k - 1], (sp, there)
        )

    for k in range(1, n_tp):
        s1_copy(k).start()
    s1[tp] = s1_src[tp]
    for j in range(1, len(pieces)):
        for k in range(1, chips):
            far_copy(k, j).start()

    fresh = nt_ref[...]
    new_gates = dot_nt(wi_ref[...], fresh)[:, :1]
    new_forgets = log_sigmoid(dot_nt(wf_ref[...], fresh)[:, :1] + shift)
    for t in range(n_tp):
        part = slice(t * heads, (t + 1) * heads)
        gnew[t, :, :128] = jnp.broadcast_to(new_gates[part], (heads, 128))
        gnew[t, :, 128:] = jnp.broadcast_to(new_forgets[part], (heads, 128))

    def product(slot, at, size):
        first = pl.multiple_of(slot * rows + at, PAD)
        for w, out in ((kw, k_out), (vw, v_out)):
            wide = min(256, w.shape[1])

            @pl.loop(0, w.shape[1] // wide)
            def _(c):
                cols = pl.ds(pl.multiple_of(c * wide, wide), wide)
                out[pl.ds(first, size), cols] = dot(
                    tok[slot, pl.ds(at, size)], w[:, cols]
                ).astype(jnp.bfloat16)

    load_kw.wait()
    load_vw.wait()
    product(tp, 0, rows)

    for k in range(1, n_tp):
        s1_copy(k).wait_recv()
    run = jnp.zeros((heads, 1), jnp.float32)
    top = jnp.full((heads, 1), -jnp.inf, jnp.float32)
    for t in reversed(range(n_tp)):
        here = s1[t, :, :rows] + run
        lwb[t] = here
        top = jnp.maximum(top, jnp.max(here, axis=1, keepdims=True))
        run = run + s1[t, :, rows : rows + 1]
    lane = lax.broadcasted_iota(jnp.int32, (heads, 128), 1)
    s2_src[...] = jnp.where(lane < 64, run, top)

    def s2_copy(k):
        return remote(
            s2_src, s2.at[sp], s2_send.at[k - 1], s2_recv.at[k - 1], ((sp + k) % n_sp, tp)
        )

    for k in range(1, n_sp):
        s2_copy(k).start()
    s2[sp] = s2_src[...]

    near.wait_recv()
    product(mate, 0, rows)

    for k in range(1, n_sp):
        s2_copy(k).wait_recv()
    run = jnp.zeros((heads, 1), jnp.float32)
    carried = jnp.zeros((heads, 1), jnp.float32)
    peak = jnp.full((heads, 1), -jnp.inf, jnp.float32)
    for b in reversed(range(n_sp)):
        peak = jnp.maximum(peak, s2[b, :, 64:65] + run)
        carried = jnp.where(b == sp, run, carried)
        run = run + s2[b, :, 0:1]
    new_gate = gnew[tp, :, 0:1]
    new_forget = gnew[tp, :, 128:129]
    stable = jnp.maximum(new_forget + peak, new_gate)
    for t in range(n_tp):
        log_weight = lwb[t] + carried
        cw_out[:, t * rows : (t + 1) * rows] = jnp.exp(log_weight - peak)
        wexp[t] = jnp.exp(new_forget + log_weight - stable)

    scale = 1.0 / math.sqrt(DQK)
    key_cols, value_cols = kw.shape[1], vw.shape[1]
    owner = lax.broadcasted_iota(jnp.int32, (heads, key_cols), 1) // DQK
    head = lax.broadcasted_iota(jnp.int32, (heads, key_cols), 0)
    query = jnp.where(
        owner == head, jnp.broadcast_to(nq_ref[...].astype(jnp.float32), (heads, key_cols)), 0.0
    )
    query_low = query.astype(jnp.bfloat16)
    which = lax.broadcasted_iota(jnp.int32, (heads, DV), 0)

    def own_columns(wide):
        found = jnp.zeros((heads, DV), jnp.float32)
        for h in range(heads):
            found = found + jnp.where(which == h, wide[:, h * DV : (h + 1) * DV], 0.0)
        return found

    new_key = dot(fresh, kw[...])[:1].astype(jnp.bfloat16).astype(jnp.float32)
    new_score = jnp.sum(query * new_key, axis=1, keepdims=True) * scale
    new_value = dot(fresh, vw[...])[:heads].astype(jnp.bfloat16).astype(jnp.float32)
    own_term = jnp.exp(new_gate - stable) * new_score
    own_value = own_term * own_columns(new_value)

    numer = jnp.zeros((heads, value_cols), jnp.float32)
    denom = jnp.zeros((heads, 1), jnp.float32)

    def read(slot, at, size, numer, denom):
        first = pl.multiple_of(slot * rows + at, PAD)
        score = dot_nt(query_low, k_out[pl.ds(first, size)]) * scale
        weighted = wexp[slot, :, at : at + size] * score
        numer = numer + dot(weighted.astype(jnp.bfloat16), v_out[pl.ds(first, size)])
        return numer, denom + jnp.sum(weighted, axis=1, keepdims=True)

    numer, denom = read(tp, 0, rows, numer, denom)
    numer, denom = read(mate, 0, rows, numer, denom)

    last = len(pieces) - 1
    for j, (at, size) in enumerate(pieces):
        for k in range(1, chips):
            far_copy(k, j).wait_recv()
            forward_copy(k, j).start()
            product(came_from(k) * 2 + core, at, size)
        for k in range(1, chips):
            forward_copy(k, j).wait_recv()
            product(came_from(k) * 2 + 1 - core, at, size)
        if j == 0 or j == last:
            start, count = (0, rows // 2) if j == 0 else (rows // 2, rows // 2)
            for k in range(1, chips):
                for side in (core, 1 - core):
                    numer, denom = read(came_from(k) * 2 + side, start, count, numer, denom)

    s3_src[:, :DV] = own_columns(numer)
    s3_src[:, DV:] = jnp.broadcast_to(denom, (heads, 128))

    def s3_copy(k):
        return remote(
            s3_src, s3.at[sp], s3_send.at[k - 1], s3_recv.at[k - 1], ((sp + k) % n_sp, tp)
        )

    for k in range(1, n_sp):
        s3_copy(k).start()
    s3[sp] = s3_src[...]
    near.wait_send()
    for j in range(len(pieces)):
        for k in range(1, chips):
            far_copy(k, j).wait_send()
            forward_copy(k, j).wait_send()
    for k in range(1, n_tp):
        s1_copy(k).wait_send()
    for k in range(1, n_sp):
        s2_copy(k).wait_send()
    for k in range(1, n_sp):
        s3_copy(k).wait_recv()
    gathered = s3[0]
    for b in range(1, n_sp):
        gathered = gathered + s3[b]
    numerator = gathered[:, :DV] + own_value
    denominator = gathered[:, DV : DV + 1] + own_term
    rd_out[...] = numerator / jnp.maximum(jnp.abs(denominator), 1.0)
    for k in range(1, n_sp):
        s3_copy(k).wait_send()


def body(
    n_sp,
    n_tp,
    prompt_tokens,
    key_weight,
    value_weight,
    input_weight,
    forget_weight,
    forget_bias,
    new_token,
    new_query,
):
    rows, depth = prompt_tokens.shape
    key_cols, value_cols = key_weight.shape[1], value_weight.shape[1]
    heads = key_cols // DQK
    block = rows * n_tp
    steps = len(pieces_of(rows))
    chips = n_tp // 2
    vmem = pl.BlockSpec(memory_space=pltpu.VMEM)
    hbm = pl.BlockSpec(memory_space=pl.ANY)
    dma = pltpu.SemaphoreType.DMA
    f32, bf16 = jnp.float32, jnp.bfloat16
    keys, values, weights, reading = pl.pallas_call(
        functools.partial(kernel, n_sp, n_tp),
        out_shape=(
            jax.ShapeDtypeStruct((block, key_cols), bf16),
            jax.ShapeDtypeStruct((block, value_cols), bf16),
            jax.ShapeDtypeStruct((heads, block), f32),
            jax.ShapeDtypeStruct((heads, DV), f32),
        ),
        in_specs=[hbm] * 3 + [vmem] * 5,
        out_specs=(vmem,) * 4,
        scratch_shapes=[
            pltpu.VMEM((n_tp, rows, depth), bf16),
            pltpu.VMEM((depth, key_cols), bf16),
            pltpu.VMEM((depth, value_cols), bf16),
            pltpu.VMEM((n_tp, heads, 256), f32),
            pltpu.VMEM((n_tp, heads, rows + 128), f32),
            pltpu.VMEM((n_tp, heads, rows + 128), f32),
            pltpu.VMEM((heads, 128), f32),
            pltpu.VMEM((n_sp, heads, 128), f32),
            pltpu.VMEM((heads, DV + 128), f32),
            pltpu.VMEM((n_sp, heads, DV + 128), f32),
            pltpu.VMEM((n_tp, heads, rows), f32),
            pltpu.VMEM((n_tp, heads, rows), f32),
            dma((3,)),
            dma((2,)),
            dma((chips - 1, steps)),
            dma((chips - 1, steps)),
            dma((chips - 1, steps)),
            dma((chips - 1, steps)),
            dma((n_tp - 1,)),
            dma((n_tp - 1,)),
            dma((n_sp - 1,)),
            dma((n_sp - 1,)),
            dma((n_sp - 1,)),
            dma((n_sp - 1,)),
        ],
        compiler_params=pltpu.CompilerParams(collective_id=0, has_side_effects=True),
    )(
        prompt_tokens,
        key_weight,
        value_weight,
        input_weight.T,
        forget_weight.T,
        forget_bias[None, :],
        jnp.broadcast_to(new_token[None, :], (PAD, depth)),
        new_query[None, :],
    )
    return keys, values, weights, reading.reshape(-1)


def solution(mesh):
    placed = (P(("sp", "tp"), None), P(None, "tp"), P(None, "tp"), P(), P(), P(), P(), P("tp"))
    return jax.shard_map(
        functools.partial(body, mesh.shape["sp"], mesh.shape["tp"]),
        mesh=mesh,
        in_specs=placed,
        out_specs=(P("sp", "tp"), P("sp", "tp"), P("tp", "sp"), P("tp")),
        check_vma=False,
    )
```

time: 139 us -> 54.3 us (0.39)
  blocking collectives: 57.8 us -> 0 us
  Pallas kernels: 0 us -> 45.9 us
  matrix products: 19.5 us -> 0 us
  waiting for transfers between devices: 18.1 us -> 0 us
  local copies, waits for them, and re-layouts: 22.2 us -> 7.53 us
  between operations: 14.8 us -> 0.65 us
  other arithmetic: 5.51 us -> 0 us
    pallas_call x0 -> x1, Pallas kernels: none -> 45.9 us  [body(): pl.pallas_call(functools.partial(kernel, n_sp, n_tp), out_shape=(jax.Shap...]
    unnamed x1 -> x0, blocking collectives: 21.3 us -> none
    dot_general x7 -> x0, matrix products: 19.5 us -> none  [the longest x1 13.5 us: body(): jnp.dot(lax.all_gather(prompt_tokens, 'tp', axis=0, tiled=True), packed,...]
    psum x1 -> x0, blocking collectives: 19.4 us -> none  [body(): numerator, denominator = lax.psum((numer_part, denom_part), 'sp')]
    all_gather x1 -> x0, waiting for transfers between devices: 17.5 us -> none  [body(): lax.all_gather(prompt_tokens, 'tp', axis=0, tiled=True)]
    pmax x1 -> x0, blocking collectives: 17.1 us -> none  [body(): peak_log = lax.pmax(jnp.max(log_weight, axis=0), 'sp')]
    concatenate x1 -> x0, local copies, waits for them, and re-layouts: 10.7 us -> none  [body(): jnp.concatenate([key_weight, value_weight, gate_input, gate_forget], axis=1)]
    broadcast_in_dim x0 -> x2, local copies, waits for them, and re-layouts: none -> 2.58 us  [the longest x1 1.32 us: body(): jnp.broadcast_to(new_token[None, :], (PAD, depth))]
  transfers between devices with their start and end apart: 1 -> 0, of which waited for: 1 -> 0; matrix products, arithmetic and copies ran while one was open for 15% -> 0% of each run, Pallas kernels for 0% -> 0%
where the time goes in v1:
time: 54.3 us; the launch traced here: 54.1 us
  Pallas kernels  45.9 us (85%)
  local copies, waits for them, and re-layouts  7.53 us (14%)
  between operations  0.65 us (1%)
    pallas_call x1, Pallas kernels, body(): pl.pallas_call(functools.partial(kernel, n_sp, n_tp), out_shape=(jax.Shap...  45.9 us
    unnamed x10, local copies, waits for them, and re-layouts  4.95 us
    broadcast_in_dim x1, local copies, waits for them, and re-layouts, body(): jnp.broadcast_to(new_token[None, :], (PAD, depth))  1.32 us
    broadcast_in_dim x1, local copies, waits for them, and re-layouts, body(): new_query[None, :]  1.26 us

profile of v1, /device:TPU:0, one launch (start us, length us, event | category | flops | bytes accessed | tf_op | source)
XLA Modules:
  0.0 54.1 jit_solution(5223985461268100270)
XLA Ops:
  0.6 1.3 %broadcast_in_dim.14.nq_ref = bf16[1,512]{1,0:T(2,128)(2,1)} reshape(bf16[512]{0:T(512)(128)(2,1)} %param.15) | data formatting | bytes 2048 | tf_op jit(solution)/shard_map/broadcast_in_dim | solution.py:391
  1.9 1.3 %broadcast_in_dim.13.nt_ref = bf16[16,2048]{1,0:T(8,128)(2,1)} broadcast(bf16[2048]{0:T(1024)(128)(2,1)} %param.14), dimensions={1} | broadcast | bytes 69632 | tf_op jit(solution)/shard_map/broadcast_in_dim | solution.py:390
  3.2 45.9 %shard_map.111 = (bf16[1024,512]{1,0:T(8,128)(2,1)}, bf16[1024,1024]{1,0:T(8,128)(2,1)}, f32[8,1024]{1,0:T(8,128)}, f32[8,128]{1,0:T(8,128)}) custom-call(bf16[256,2048]{1,0:T(8,128)(2,1)} %tok_hbm.1, bf16[2048,512]{1,0:T(8,128)(2,1)} %kw_hbm.1, bf16[2048,1024]{1,0:T(8,128)(2,1)} %vw_hbm.1, bf16[32,2048]{1,0:T(8,128)(2,1)} %bitcast.4, ...), custom_call_target="tpu_custom_call" | custom-call | tf_op jit(solution)/shard_map/pallas_call | solution.py:346
  49.1 0.0 copy-start
  49.2 2.4 %copy.16 = bf16[1024,512]{1,0:T(8,128)(2,1)} copy(bf16[1024,512]{1,0:T(8,128)(2,1)} %get-tuple-element.16) | data formatting | bytes 2097152
  51.6 0.0 copy-done
  51.6 0.0 copy-start.1
  51.6 0.0 copy-start.2
  51.6 1.3 %copy.17 = bf16[1024,1024]{1,0:T(8,128)(2,1)} copy(bf16[1024,1024]{1,0:T(8,128)(2,1)S(1)} %copy-done) | data formatting | bytes 4194304
  52.9 0.0 copy-done.1
  52.9 0.6 %copy.18 = f32[8,1024]{1,0:T(8,128)} copy(f32[8,1024]{1,0:T(8,128)S(1)} %copy-done.1) | data formatting | bytes 65536
  53.5 0.0 copy-done.2
  53.5 0.6 %copy.19 = f32[1024]{0:T(1024)} copy(f32[1024]{0:T(1024)S(1)} %bitcast.6) | data formatting | bytes 8192
Async XLA Ops:
  49.1 2.4 %copy-start = (bf16[1024,1024]{1,0:T(8,128)(2,1)S(1)}, bf16[1024,1024]{1,0:T(8,128)(2,1)}, u32[]{:S(2)}) copy-start(bf16[1024,1024]{1,0:T(8,128)(2,1)} %get-tuple-element.17) | copy-start | bytes 6291460
  51.6 1.3 %copy-start.1 = (f32[8,1024]{1,0:T(8,128)S(1)}, f32[8,1024]{1,0:T(8,128)}, u32[]{:S(2)}) copy-start(f32[8,1024]{1,0:T(8,128)} %get-tuple-element.18) | copy-start | bytes 98308
  51.6 1.9 %copy-start.2 = (f32[8,128]{1,0:T(8,128)S(1)}, f32[8,128]{1,0:T(8,128)}, u32[]{:S(2)}) copy-start(f32[8,128]{1,0:T(8,128)} %get-tuple-element.11) | copy-start | bytes 12292

commit v2 on v1

--- a/solution.py
+++ b/solution.py
@@ -37,11 +37,11 @@
     tok_hbm,
     kw_hbm,
     vw_hbm,
-    wi_ref,
-    wf_ref,
-    fb_ref,
-    nt_ref,
-    nq_ref,
+    wi_hbm,
+    wf_hbm,
+    fb_hbm,
+    nt_hbm,
+    nq_hbm,
     k_out,
     v_out,
     cw_out,
@@ -49,6 +49,11 @@
     tok,
     kw,
     vw,
+    wi_ref,
+    wf_ref,
+    fb_ref,
+    nt_ref,
+    nq_ref,
     gnew,
     s1_src,
     s1,
@@ -80,13 +85,6 @@
     all_heads = wi_ref.shape[0]
     pieces = pieces_of(rows)
 
-    load_tok = pltpu.make_async_copy(tok_hbm, tok.at[tp], local_sem.at[0])
-    load_kw = pltpu.make_async_copy(kw_hbm, kw, local_sem.at[1])
-    load_vw = pltpu.make_async_copy(vw_hbm, vw, local_sem.at[2])
-    load_tok.start()
-    load_kw.start()
-    load_vw.start()
-
     barrier = pltpu.get_barrier_semaphore()
     for k in range(1, n_tp):
         pl.semaphore_signal(
@@ -96,6 +94,23 @@
         pl.semaphore_signal(
             barrier, inc=1, device_id=((sp + k) % n_sp, tp), device_id_type=MESH
         )
+    loads = [
+        pltpu.make_async_copy(src, dst, local_sem.at[i])
+        for i, (src, dst) in enumerate(
+            (
+                (tok_hbm, tok.at[tp]),
+                (wi_hbm, wi_ref),
+                (wf_hbm, wf_ref),
+                (fb_hbm, fb_ref),
+                (nt_hbm, nt_ref),
+                (nq_hbm, nq_ref),
+                (kw_hbm, kw),
+                (vw_hbm, vw),
+            )
+        )
+    ]
+    for load in loads:
+        load.start()
     pl.semaphore_wait(barrier, n_tp - 1 + n_sp - 1)
 
     def remote(src, dst, send, recv, device):
@@ -138,10 +153,11 @@
         far_copy(k, 0).start()
     near.start()
 
+    for load in loads[:6]:
+        load.wait()
     row_iota = lax.broadcasted_iota(jnp.int32, (all_heads, all_heads), 0)
     col_iota = lax.broadcasted_iota(jnp.int32, (all_heads, all_heads), 1)
     shift = jnp.sum(jnp.where(row_iota == col_iota, fb_ref[...], 0.0), axis=1, keepdims=True)
-    load_tok.wait()
     own = tok[tp]
     gate = dot_nt(wi_ref[...], own)
     log_forget = log_sigmoid(dot_nt(wf_ref[...], own) + shift)
@@ -174,7 +190,7 @@
         for k in range(1, chips):
             far_copy(k, j).start()
 
-    fresh = nt_ref[...]
+    fresh = jnp.broadcast_to(nt_ref[...].reshape(1, -1), (PAD, nt_ref.shape[0]))
     new_gates = dot_nt(wi_ref[...], fresh)[:, :1]
     new_forgets = log_sigmoid(dot_nt(wf_ref[...], fresh)[:, :1] + shift)
     for t in range(n_tp):
@@ -187,15 +203,21 @@
         for w, out in ((kw, k_out), (vw, v_out)):
             wide = min(256, w.shape[1])
 
-            @pl.loop(0, w.shape[1] // wide)
-            def _(c):
+            def tile(c):
                 cols = pl.ds(pl.multiple_of(c * wide, wide), wide)
                 out[pl.ds(first, size), cols] = dot(
                     tok[slot, pl.ds(at, size)], w[:, cols]
                 ).astype(jnp.bfloat16)
 
-    load_kw.wait()
-    load_vw.wait()
+            if size <= 64:
+                out[pl.ds(first, size), :] = dot(
+                    tok[slot, pl.ds(at, size)], w[...]
+                ).astype(jnp.bfloat16)
+            else:
+                pl.loop(0, w.shape[1] // wide)(tile)
+
+    for load in loads[6:]:
+        load.wait()
     product(tp, 0, rows)
 
     for k in range(1, n_tp):
@@ -244,7 +266,7 @@
     owner = lax.broadcasted_iota(jnp.int32, (heads, key_cols), 1) // DQK
     head = lax.broadcasted_iota(jnp.int32, (heads, key_cols), 0)
     query = jnp.where(
-        owner == head, jnp.broadcast_to(nq_ref[...].astype(jnp.float32), (heads, key_cols)), 0.0
+        owner == head, jnp.broadcast_to(nq_ref[...].reshape(1, -1).astype(jnp.float32), (heads, key_cols)), 0.0
     )
     query_low = query.astype(jnp.bfloat16)
     which = lax.broadcasted_iota(jnp.int32, (heads, DV), 0)
@@ -343,20 +365,26 @@
     hbm = pl.BlockSpec(memory_space=pl.ANY)
     dma = pltpu.SemaphoreType.DMA
     f32, bf16 = jnp.float32, jnp.bfloat16
+    results = (
+        ((block, key_cols), bf16),
+        ((block, value_cols), bf16),
+        ((heads, block), f32),
+        ((heads, DV), f32),
+    )
     keys, values, weights, reading = pl.pallas_call(
         functools.partial(kernel, n_sp, n_tp),
-        out_shape=(
-            jax.ShapeDtypeStruct((block, key_cols), bf16),
-            jax.ShapeDtypeStruct((block, value_cols), bf16),
-            jax.ShapeDtypeStruct((heads, block), f32),
-            jax.ShapeDtypeStruct((heads, DV), f32),
-        ),
-        in_specs=[hbm] * 3 + [vmem] * 5,
+        out_shape=tuple(pltpu.VMEM(dims, kind) for dims, kind in results),
+        in_specs=[hbm] * 8,
         out_specs=(vmem,) * 4,
         scratch_shapes=[
             pltpu.VMEM((n_tp, rows, depth), bf16),
             pltpu.VMEM((depth, key_cols), bf16),
             pltpu.VMEM((depth, value_cols), bf16),
+            pltpu.VMEM(input_weight.shape[::-1], bf16),
+            pltpu.VMEM(input_weight.shape[::-1], bf16),
+            pltpu.VMEM((1,) + forget_bias.shape, f32),
+            pltpu.VMEM(new_token.shape, bf16),
+            pltpu.VMEM(new_query.shape, bf16),
             pltpu.VMEM((n_tp, heads, 256), f32),
             pltpu.VMEM((n_tp, heads, rows + 128), f32),
             pltpu.VMEM((n_tp, heads, rows + 128), f32),
@@ -366,7 +394,7 @@
             pltpu.VMEM((n_sp, heads, DV + 128), f32),
             pltpu.VMEM((n_tp, heads, rows), f32),
             pltpu.VMEM((n_tp, heads, rows), f32),
-            dma((3,)),
+            dma((8,)),
             dma((2,)),
             dma((chips - 1, steps)),
             dma((chips - 1, steps)),
@@ -387,8 +415,8 @@
         input_weight.T,
         forget_weight.T,
         forget_bias[None, :],
-        jnp.broadcast_to(new_token[None, :], (PAD, depth)),
-        new_query[None, :],
+        new_token,
+        new_query,
     )
     return keys, values, weights, reading.reshape(-1)
 

time: 54.3 us -> 44.9 us (0.83)
  Pallas kernels: 45.9 us -> 40.6 us
  local copies, waits for them, and re-layouts: 7.53 us -> 3.5 us
    pallas_call x1, Pallas kernels: 45.9 us -> 40.6 us  [body(): pl.pallas_call(functools.partial(kernel, n_sp, n_tp), out_shape=tuple((pl...]
    broadcast_in_dim x2 -> x0, local copies, waits for them, and re-layouts: 2.58 us -> none  [the longest x1 1.32 us: body(): jnp.broadcast_to(new_token[None, :], (PAD, depth))]
    unnamed x10 -> x4, local copies, waits for them, and re-layouts: 4.95 us -> 3.5 us
where the time goes in v2:
time: 44.9 us; the launch traced here: 44.8 us
  Pallas kernels  40.6 us (90%)
  local copies, waits for them, and re-layouts  3.5 us (8%)
  between operations  0.64 us (1%)
    pallas_call x1, Pallas kernels, body(): pl.pallas_call(functools.partial(kernel, n_sp, n_tp), out_shape=tuple((pl...  40.6 us
    unnamed x4, local copies, waits for them, and re-layouts  3.5 us

profile of v2, /device:TPU:0, one launch (start us, length us, event | category | flops | bytes accessed | tf_op | source)
XLA Modules:
  0.0 44.8 jit_solution(12568087010162146078)
XLA Ops:
  0.6 40.6 %shard_map.111 = (bf16[1024,512]{1,0:T(8,128)(2,1)S(1)}, bf16[1024,1024]{1,0:T(8,128)(2,1)S(1)}, f32[8,1024]{1,0:T(8,128)S(1)}, f32[8,128]{1,0:T(8,128)S(1)}) custom-call(bf16[256,2048]{1,0:T(8,128)(2,1)} %tok_hbm.1, bf16[2048,512]{1,0:T(8,128)(2,1)} %kw_hbm.1, bf16[2048,1024]{1,0:T(8,128)(2,1)} %vw_hbm.1, bf16[32,2048]{1,0:T(8,128)(2,1)} %bitcast.5, ...), custom_call_target="tpu_custom_call" | custom-call | tf_op jit(solution)/shard_map/pallas_call | solution.py:374
  41.3 1.0 %copy.16 = bf16[1024,512]{1,0:T(8,128)(2,1)} copy(bf16[1024,512]{1,0:T(8,128)(2,1)S(1)} %get-tuple-element.12) | data formatting | bytes 2097152
  42.3 0.6 %copy.19 = f32[1024]{0:T(1024)} copy(f32[1024]{0:T(1024)S(1)} %bitcast.4) | data formatting | bytes 8192
  42.9 0.6 %copy.18 = f32[8,1024]{1,0:T(8,128)} copy(f32[8,1024]{1,0:T(8,128)S(1)} %get-tuple-element.14) | data formatting | bytes 65536
  43.5 1.3 %copy.17 = bf16[1024,1024]{1,0:T(8,128)(2,1)} copy(bf16[1024,1024]{1,0:T(8,128)(2,1)S(1)} %get-tuple-element.13) | data formatting | bytes 4194304
